TPU v7x, 32 devices: a whole 2x2x4 slice. The times are simulated.
32 devices in a mesh: grp: 2 (over y), ep: 4 (over z), tp: 4 (over x, core).
Axes of the slice: x: 2, y: 2, z: 4, core: 2. Of those that a mesh axis runs over, the one named last changes fastest.
Arguments:
- queries: bfloat16 [3072, 1024], P(('grp', 'ep'), 'tp'), parts along dimension 0, may hold values from -6 to 6
- key_values: bfloat16 [3072, 512], P(('grp', 'ep'), 'tp'), parts along dimension 0, may hold values from -6 to 6
- query_gain: float32 [64], replicated, may hold values from 0.5 to 5
- key_gain: float32 [64], replicated, may hold values from 0.5 to 5
- out_weight: bfloat16 [1024, 2048], P('tp'), may hold values from -0.1875 to 0.1875
- second_batch: bfloat16 [4096, 2048], P(('grp', 'ep', 'tp')), parts along dimension 0, may hold values from -6 to 6
- norm_gain: float32 [2048], replicated, may hold values from 0.1 to 1.9
- routes: int32 [4096, 2], P(('grp', 'ep', 'tp')), parts along dimension 0, may hold values from 0 to 7, all different within a row; in each aligned block of 128 rows (0 to 127, 128 to 255, ...) at most 48 rows name the same one
- route_weights: float32 [4096, 2], P(('grp', 'ep', 'tp')), parts along dimension 0, may hold values from 0.2 to 1
- expert_gate: bfloat16 [8, 2048, 1024], P('ep', None, 'tp'), may hold values from -0.125 to 0.125
- expert_up: bfloat16 [8, 2048, 1024], P('ep', None, 'tp'), may hold values from -0.125 to 0.125
- expert_down: bfloat16 [8, 1024, 2048], P('ep', 'tp'), may hold values from -0.1875 to 0.1875
- shared_gate: bfloat16 [2048, 512], P(None, 'tp'), may hold values from -0.125 to 0.125
- shared_up: bfloat16 [2048, 512], P(None, 'tp'), may hold values from -0.125 to 0.125
- shared_down: bfloat16 [512, 2048], P('tp'), may hold values from -0.25 to 0.25
Outputs:
- mixer_out: bfloat16 [3072, 2048], P(('grp', 'ep', 'tp')), parts along dimension 0
- channel_out: bfloat16 [4096, 2048], P(('grp', 'ep', 'tp')), parts along dimension 0
There are 2 independent parts, one for each index of `grp`. A program takes and returns all parts, laid end to end along the dimension named above; an argument that names none is the same for every part. Nothing has to cross between parts.
Inputs may be any that keep to these rules, and one draw needn't show every extreme that they name: `routes`: each row names 2 different experts. Among the rows of one device no expert is named more than 48 times, and in every draw some expert is named exactly 48 times by the rows of some device.
All inputs are finite; a program needn't handle non-finite values.
Results may differ from a plain program's by a relative error of at most 0.015.
The roundings to bfloat16 on the way count: a program that leaves them out, or rounds other values in their place, can miss the bound.
Values may be sent and summed in bfloat16 or wider, within the bound.
A program may use at most 128 MiB of HBM per device.

v0:
```python
import jax
import jax.numpy as jnp
from jax import lax
from jax.sharding import PartitionSpec as P

GRID_W = 64
rope_base = 10000.0
norm_eps = 1e-06


def head_norm(vectors, gain):
    return (
        vectors * lax.rsqrt(jnp.mean(vectors * vectors, axis=-1, keepdims=True) + norm_eps) * gain
    )


def turn_heads(vectors, positions):
    row_count, head_count, head_size = vectors.shape
    half_size = head_size // 2
    inverse = rope_base ** (-jnp.arange(0, half_size, 2, dtype=jnp.float32) / half_size)
    grid_row = (positions // GRID_W).astype(jnp.float32)
    grid_column = (positions % GRID_W).astype(jnp.float32)
    angles = jnp.concatenate([grid_row[:, None] * inverse, grid_column[:, None] * inverse], axis=-1)
    cosine = jnp.cos(angles)[:, None, :]
    sine = jnp.sin(angles)[:, None, :]
    paired = vectors.reshape(row_count, head_count, half_size, 2)
    first = paired[..., 0]
    second = paired[..., 1]
    turned = jnp.stack([first * cosine - second * sine, first * sine + second * cosine], axis=-1)
    return turned.reshape(vectors.shape)


def slot_ids(route_rows, expert_count, capacity):
    row_count, top_count = route_rows.shape
    flat_routes = route_rows.reshape(-1)
    onehot = (flat_routes[:, None] == jnp.arange(expert_count, dtype=jnp.int32)[None, :]).astype(
        jnp.int32
    )
    earlier = jnp.cumsum(onehot, axis=0) - onehot
    within = jnp.sum(earlier * onehot, axis=1)
    return (flat_routes * capacity + within).reshape(row_count, top_count)


def slot_table(slots, slot_count):
    row_count, top_count = slots.shape
    flat_slots = slots.reshape(-1)
    owner_row = jnp.arange(row_count * top_count, dtype=jnp.int32) // top_count
    matches = flat_slots[None, :] == jnp.arange(slot_count, dtype=jnp.int32)[:, None]
    occupied = jnp.any(matches, axis=1)
    source_row = jnp.sum(jnp.where(matches, owner_row[None, :], 0), axis=1)
    return jnp.where(occupied, source_row, row_count)


def pick_block(row_count):
    for candidate in range(min(row_count, 1024), 0, -1):
        if row_count % candidate == 0:
            return candidate
    return row_count


def attend_keys(query_turned, scale, running, pieces):
    head_size = query_turned.shape[-1]
    key_block = pick_block(pieces.shape[0])
    blocks = pieces.reshape(pieces.shape[0] // key_block, key_block, 2 * head_size)

    def one_block(carried, block_rows):
        top_now, total_now, acc_now = carried
        scores = (
            jnp.einsum(
                "qhd,kd->hqk",
                query_turned,
                block_rows[:, :head_size],
                preferred_element_type=jnp.float32,
            )
            * scale
        )
        top_new = jnp.maximum(top_now, jnp.max(scores, axis=-1))
        shrink = jnp.exp(top_now - top_new)
        exps = jnp.exp(scores - top_new[..., None])
        total_new = total_now * shrink + jnp.sum(exps, axis=-1)
        acc_new = acc_now * shrink[..., None] + jnp.einsum(
            "hqk,kd->hqd",
            exps.astype(jnp.bfloat16),
            block_rows[:, head_size:],
            preferred_element_type=jnp.float32,
        )
        return ((top_new, total_new, acc_new), None)

    result, ignored = lax.scan(one_block, running, blocks)
    return result


def shared_hidden_of(token_rows, gate_weights, up_weights):
    gate_part = jnp.dot(token_rows, gate_weights, preferred_element_type=jnp.float32)
    up_part = jnp.dot(token_rows, up_weights, preferred_element_type=jnp.float32)
    return (jax.nn.silu(gate_part) * up_part).astype(jnp.bfloat16)


def expert_hidden(slot_rows, gate_weights, up_weights):
    gate_part = jnp.einsum(
        "osjcd,jdf->osjcf", slot_rows, gate_weights, preferred_element_type=jnp.float32
    )
    up_part = jnp.einsum(
        "osjcd,jdf->osjcf", slot_rows, up_weights, preferred_element_type=jnp.float32
    )
    return (jax.nn.silu(gate_part) * up_part).astype(jnp.bfloat16)


def body(
    queries,
    key_values,
    query_gain,
    key_gain,
    out_weight,
    second_batch,
    norm_gain,
    routes,
    route_weights,
    expert_gate,
    expert_up,
    expert_down,
    shared_gate,
    shared_up,
    shared_down,
):
    query_rows = queries.shape[0]
    head_size = query_gain.shape[0]
    heads_here = queries.shape[1] // head_size
    ep_count = lax.axis_size("ep")
    positions = lax.axis_index("ep") * query_rows + jnp.arange(query_rows, dtype=jnp.int32)
    query_turned = turn_heads(
        head_norm(
            queries.reshape(query_rows, heads_here, head_size).astype(jnp.float32), query_gain
        ),
        positions,
    ).astype(jnp.bfloat16)
    key_turned = turn_heads(
        head_norm(key_values[:, None, :head_size].astype(jnp.float32), key_gain), positions
    ).astype(jnp.bfloat16)
    keys_and_values = jnp.concatenate([key_turned[:, 0, :], key_values[:, head_size:]], axis=1)
    start_state = (
        jnp.full((heads_here, query_rows), -1e30, jnp.float32),
        jnp.zeros((heads_here, query_rows), jnp.float32),
        jnp.zeros((heads_here, query_rows, head_size), jnp.float32),
    )
    top_all, total_all, acc_all = attend_keys(
        query_turned,
        head_size ** (-0.5),
        start_state,
        lax.all_gather(keys_and_values, "ep", axis=0, tiled=True),
    )
    head_out = (
        (acc_all / total_all[..., None])
        .transpose(1, 0, 2)
        .reshape(query_rows, heads_here * head_size)
        .astype(jnp.bfloat16)
    )
    tok_count = second_batch.shape[0]
    model_width = second_batch.shape[1]
    top_count = routes.shape[1]
    local_experts = expert_gate.shape[0]
    expert_count = local_experts * ep_count
    capacity = 3 * tok_count * top_count // (2 * expert_count)
    slot_count = expert_count * capacity
    token_float = second_batch.astype(jnp.float32)
    normed = (
        token_float
        * lax.rsqrt(jnp.mean(token_float * token_float, axis=-1, keepdims=True) + norm_eps)
        * norm_gain
    ).astype(jnp.bfloat16)
    own_slots = slot_ids(routes, expert_count, capacity)
    shared_hidden = shared_hidden_of(
        lax.all_gather(normed, "tp", axis=0, tiled=True), shared_gate, shared_up
    )
    outgoing = jnp.take(
        normed, slot_table(own_slots, slot_count), axis=0, mode="fill", fill_value=0
    )[None]
    arrived = lax.all_to_all(outgoing, "ep", split_axis=1, concat_axis=1, tiled=True)
    arrived = arrived.reshape(arrived.shape[0], ep_count, local_experts, capacity, model_width)
    hidden = expert_hidden(
        lax.all_gather(arrived, "tp", axis=0, tiled=True), expert_gate, expert_up
    )
    routed_part = jnp.einsum(
        "osjcf,jfd->osjcd", hidden, expert_down, preferred_element_type=jnp.float32
    ).reshape(-1, model_width)
    shared_part = jnp.dot(shared_hidden, shared_down, preferred_element_type=jnp.float32)
    head_partial = jnp.dot(head_out, out_weight, preferred_element_type=jnp.float32)
    attn_sum, routed_sum, shared_sum = (
        lax.psum_scatter(
            head_partial.astype(jnp.bfloat16), "tp", scatter_dimension=0, tiled=True
        ).astype(jnp.float32),
        lax.psum_scatter(
            routed_part.astype(jnp.bfloat16), "tp", scatter_dimension=0, tiled=True
        ).astype(jnp.float32),
        lax.psum_scatter(
            shared_part.astype(jnp.bfloat16), "tp", scatter_dimension=0, tiled=True
        ).astype(jnp.float32),
    )
    returned = lax.all_to_all(
        routed_sum.astype(jnp.bfloat16), "ep", split_axis=0, concat_axis=0, tiled=True
    )
    combined = shared_sum
    for slot_pick in range(top_count):
        combined = combined + route_weights[:, slot_pick : slot_pick + 1] * jnp.take(
            returned, own_slots[:, slot_pick], axis=0
        ).astype(jnp.float32)
    return (attn_sum.astype(jnp.bfloat16), combined.astype(jnp.bfloat16))


def solution(mesh):
    placed = (
        P(("grp", "ep"), "tp"),
        P(("grp", "ep"), "tp"),
        P(),
        P(),
        P("tp", None),
        P(("grp", "ep", "tp"), None),
        P(),
        P(("grp", "ep", "tp"), None),
        P(("grp", "ep", "tp"), None),
        P("ep", None, "tp"),
        P("ep", None, "tp"),
        P("ep", "tp", None),
        P(None, "tp"),
        P(None, "tp"),
        P("tp", None),
    )
    return jax.shard_map(
        body,
        mesh=mesh,
        in_specs=placed,
        out_specs=(P(("grp", "ep", "tp"), None), P(("grp", "ep", "tp"), None)),
        check_vma=False,
    )
```

profile of v0, /device:TPU:0, one launch (start us, length us, event | category | flops | bytes accessed | tf_op | source)
XLA Modules:
  0.0 293.0 jit_solution(5934166044517611856)
XLA Ops:
  7.2 0.9 copy.85
  8.4 0.6 reduce-window.6
  9.0 0.2 slice_reduce_fusion
  9.8 1.2 fusion.25
  11.0 1.2 fusion.27
  12.2 3.1 %gather_fusion = bf16[384,2048]{1,0:T(8,128)(2,1)} fusion(bf16[128,2048]{1,0:T(8,128)(2,1)S(1)} %fusion.27, s32[1024]{0:T(1024)S(1)} %pad_clamp_fusion.2), kind=kCustom, calls=%fused_computation.2 | custom fusion | bytes 3147264 | tf_op jit(solution)/shard_map/jit(_take)/gather | solution.py:175
  15.4 1.6 bitcast_select_fusion
  17.0 4.1 %copy.106 = bf16[1,384,2048]{2,0,1:T(2,128)(2,1)} copy(bf16[1,384,2048]{2,1,0:T(8,128)(2,1)S(1)} %bitcast_select_fusion) | data formatting | bytes 3145728 | tf_op jit(solution)/shard_map/jit(_take)/select_n | solution.py:175
  21.0 0.5 broadcast.414
  21.5 12.4 %reduce.6 = bf16[384,2048]{1,0:T(8,128)(2,1)} reduce(bf16[384,1,2048]{2,1,0:T(2,128)(2,1)} %bitcast.138, bf16[]{:T(256)} %broadcast.414), dimensions={1}, to_apply=%bitcast.118.reduce_sub_computation | reduce | bytes 3145730
  33.9 4.1 %reshape.479 = bf16[4,2,98304]{2,1,0:T(2,128)(2,1)} reshape(bf16[384,2048]{1,0:T(8,128)(2,1)} %reduce.6) | data formatting | bytes 3145728
  38.0 43.4 %all_to_all.17 = bf16[4,2,98304]{2,1,0:T(2,128)(2,1)} all-to-all(bf16[4,2,98304]{2,1,0:T(2,128)(2,1)} %reshape.479), channel_id=1, replica_groups=mesh['grp'=2,'ep'=4,'tp'=4] {'ep'}, dimensions={0} | all-to-all | bytes 3145728 | tf_op jit(solution)/shard_map/all_to_all | solution.py:178
  81.4 4.5 %reshape.480 = bf16[384,1,2048]{2,1,0:T(2,128)(2,1)} reshape(bf16[4,2,98304]{2,1,0:T(2,128)(2,1)} %all_to_all.17) | data formatting | bytes 3145728
  85.9 2.8 copy.96
  88.7 1.3 copy.89
  90.1 0.7 all-gather.3.cloned.1.call-update
  90.9 44.9 %all-gather.5.cloned.1.call-done = bf16[4,4,2,48,2048]{4,3,1,0,2:T(8,128)(2,1)} async-done(((bf16[1,4,2,48,2048]{4,3,1,0,2:T(8,128)(2,1)}), bf16[4,4,2,48,2048]{4,3,1,0,2:T(8,128)(2,1)}) %all-gather.5.cloned.1.call-update) | async-done | bytes 6291472 | tf_op jit(solution)/shard_map/all_gather | solution.py:181
  135.7 6.4 %fusion.14 = f32[2,4,4,48,256]{4,3,2,1,0:T(8,128)} fusion(bf16[4,4,2,48,2048]{4,3,1,0,2:T(8,128)(2,1)} %all-gather.5.cloned.1.call-done, bf16[2,2048,256]{2,1,0:T(8,128)(2,1)} %param.28), kind=kOutput, calls=%fused_computation.26 | convolution fusion | flops 1610612736 | bytes 9961472 | tf_op jit(solution)/shard_map/osjcd,jdf->osjcf/dot_general | solution.py:100
  142.1 10.7 %convert_bitcast_fusion = bf16[4,4,2,48,2048]{4,3,1,0,2:T(8,128)(2,1)} fusion(bf16[2,256,2048]{2,1,0:T(8,128)(2,1)S(1)} %copy-done, f32[2,4,4,48,256]{4,3,2,1,0:T(8,128)} %fusion.14, bf16[4,4,2,48,2048]{4,3,1,0,2:T(8,128)(2,1)} %all-gather.5.cloned.1.call-done, bf16[2,2048,256]{2,1,0:T(8,128)(2,1)} %param.29), kind=kOutput, calls=%fused_computation.20 | convolution fusion | flops 3226730496 | bytes 18350080 | tf_op jit(solution)/shard_map/osjcf,jfd->osjcd/dot_general | solution.py:183
  152.9 6.6 %copy.90 = bf16[4,4,2,48,2048]{4,3,2,1,0:T(8,128)(2,1)} copy(bf16[4,4,2,48,2048]{4,3,1,0,2:T(8,128)(2,1)} %convert_bitcast_fusion) | data formatting | bytes 12582912 | tf_op jit(solution)/shard_map/convert_element_type | solution.py:193
  159.5 0.8 copy-done.9
  161.7 0.2 subtract_convert_fusion.1
  161.9 0.2 multiply_multiply_fusion
  162.2 0.5 subtract_convert_fusion
  162.7 2.4 fusion.57
  165.2 4.9 %convolution_convert_fusion = bf16[512,2048]{1,0:T(8,128)(2,1)} fusion(bf16[128,2048]{1,0:T(8,128)(2,1)} %param.33, bf16[512,2048]{1,0:T(8,128)(2,1)S(1)} %copy-done.5, bf16[2048,128]{1,0:T(8,128)(2,1)} %param.32, f32[512,128]{1,0:T(8,128)S(1)} %fusion.57), kind=kOutput, calls=%fused_computation.21 | convolution fusion | flops 538312704 | bytes 5505024 | tf_op jit(solution)/shard_map/dot_general | solution.py:186
  170.1 0.3 reduce-scatter.4.cloned.1.call-start
  170.3 0.4 pad_maximum_fusion
  171.1 14.6 %all_gather.9 = bf16[1536,128]{0,1:T(8,128)(2,1)S(1)} all-gather(bf16[384,128]{0,1:T(8,128)(2,1)S(1)} %pad_maximum_fusion.1), channel_id=1, replica_groups=mesh['grp'=2,'ep'=4,'tp'=4] {'ep'}, dimensions={0}, use_global_device_ids=true | all-gather | bytes 491520 | tf_op jit(solution)/shard_map/all_gather | solution.py:150
  185.7 0.2 copy.82
  185.9 15.9 %while.15 = (s32[]{:T(128)}, f32[4,384]{1,0:T(4,128)S(1)}, f32[4,384]{1,0:T(4,128)S(1)}, f32[4,384,64]{1,2,0:T(8,128)S(1)}, bf16[2,768,128]{2,1,0:T(8,128)(2,1)S...) while((s32[]{:T(128)}, f32[4,384]{1,0:T(4,128)S(1)}, f32[4,384]{1,0:T(4,128)S(1)}, ...), condition=%wide.region_5.6_spmd.clone, body=%wide.region_2.5_spmd.clone.sunk | while | flops 311729664 | bytes 35094656 | solution.py:89
  186.1 3.0 %bitcast_reduce_fusion.3 = (f32[4,384]{1,0:T(4,128)S(1)}, f32[768,384,4]{1,0,2:T(8,128)}) fusion(bf16[384,4,64]{0,2,1:T(8,128)(2,1)S(1)} %get-tuple-element.203, bf16[768,128]{0,1:T(8,128)(2,1)S(1)} %bitcast.136), kind=kOutput, calls=%fused_computation.4.clone.1 | convolution fusion | flops 153352704 | bytes 5019648 | tf_op jit(solution)/shard_map/while/body/eval_jaxpr/qhd,kd->hqk/dot_general | solution.py:69
  189.1 3.3 %fusion.75 = f32[4,384]{1,0:T(4,128)S(1)} fusion(f32[768,384,4]{1,0,2:T(8,128)} %get-tuple-element.179, f32[4,384]{1,0:T(4,128)S(1)} %select_maximum_fusion.2), kind=kLoop, calls=%fused_computation.7.clone.1 | loop fusion | flops 3537408 | bytes 4730880 | tf_op jit(solution)/shard_map/while/body/eval_jaxpr/reduce_sum | solution.py:80
  192.4 0.5 copy-done.2
  192.9 1.0 fusion.77
  194.1 3.0 %bitcast_reduce_fusion.3 = (f32[4,384]{1,0:T(4,128)S(1)}, f32[768,384,4]{1,0,2:T(8,128)}) fusion(bf16[384,4,64]{0,2,1:T(8,128)(2,1)S(1)} %get-tuple-element.203, bf16[768,128]{0,1:T(8,128)(2,1)S(1)} %bitcast.136), kind=kOutput, calls=%fused_computation.4.clone.1 | convolution fusion | flops 153352704 | bytes 5019648 | tf_op jit(solution)/shard_map/while/body/eval_jaxpr/qhd,kd->hqk/dot_general | solution.py:69
  197.1 3.3 %fusion.75 = f32[4,384]{1,0:T(4,128)S(1)} fusion(f32[768,384,4]{1,0,2:T(8,128)} %get-tuple-element.179, f32[4,384]{1,0:T(4,128)S(1)} %select_maximum_fusion.2), kind=kLoop, calls=%fused_computation.7.clone.1 | loop fusion | flops 3537408 | bytes 4730880 | tf_op jit(solution)/shard_map/while/body/eval_jaxpr/reduce_sum | solution.py:80
  200.4 0.5 copy-done.2
  200.8 1.0 fusion.77
  201.9 1.8 convolution_convert_fusion.1
  203.7 18.2 %reduce-scatter.8.cloned.1.call-done = bf16[384,2048]{1,0:T(8,128)(2,1)} async-done(((bf16[1536,2048]{1,0:T(8,128)(2,1)}), bf16[384,2048]{1,0:T(8,128)(2,1)}) %reduce-scatter.8.cloned.1.call-update) | async-done | bytes 1572880 | tf_op jit(solution)/shard_map/reduce_scatter | solution.py:192
  221.9 4.6 %all-to-all-start.1 = ((bf16[4,96,2048]{2,1,0:T(8,128)(2,1)}), bf16[4,96,2048]{2,1,0:T(8,128)(2,1)S(1)}, u32[]{:S(2)}, u32[]{:S(2)}) async-start(bf16[4,96,2048]{2,1,0:T(8,128)(2,1)} %bitcast.142), calls=%async_computation.4 | async-start | bytes 3145728 | tf_op jit(solution)/shard_map/all_to_all | solution.py:199
  226.8 36.5 %all-to-all-done.1 = bf16[4,96,2048]{2,1,0:T(8,128)(2,1)S(1)} async-done(((bf16[4,96,2048]{2,1,0:T(8,128)(2,1)}), bf16[4,96,2048]{2,1,0:T(8,128)(2,1)S(1)}, u32[]{:S(2)}, u32[]{:S(2)}) %all-to-all-start.1) | async-done | bytes 1572896 | tf_op jit(solution)/shard_map/all_to_all | solution.py:199
  263.3 0.9 gather_fusion.1
  264.2 0.3 copy-done.4
  264.5 3.4 %gather_fusion.2 = bf16[128,2048]{1,0:T(8,128)(2,1)S(1)} fusion(bf16[384,2048]{1,0:T(8,128)(2,1)} %bitcast.134, s32[1024]{0:T(1024)S(1)} %get-tuple-element.135), kind=kCustom, calls=%fused_computation.1.clone | custom fusion | bytes 1049088 | tf_op jit(solution)/shard_map/jit(_take)/gather | solution.py:204
  267.9 2.3 add_convert_fusion
  270.2 16.3 %reduce-scatter.4.cloned.1.call-done = bf16[96,2048]{1,0:T(8,128)(2,1)} async-done(((bf16[384,2048]{1,0:T(8,128)(2,1)}), bf16[96,2048]{1,0:T(8,128)(2,1)}) %reduce-scatter.4.cloned.1.call-update) | async-done | bytes 393232 | tf_op jit(solution)/shard_map/reduce_scatter | solution.py:189
  (91 shorter events, 3.3 us)
Async XLA Ops:
  7.2 135.0 %copy-start = (bf16[2,256,2048]{2,1,0:T(8,128)(2,1)S(1)}, bf16[2,256,2048]{2,1,0:T(8,128)(2,1)}, u32[]{:S(2)}) copy-start(bf16[2,256,2048]{2,1,0:T(8,128)(2,1)} %param.30) | copy-start | bytes 6291460
  7.2 128.6 %all-gather.5.cloned.1.call-start = ((), (), s32[]{:S(2)}) async-start(), calls=%async_computation.8 | async-start | bytes 7864320 | tf_op jit(solution)/shard_map/all_gather | solution.py:181
  12.2 3.1 %copy-start.3 = (bf16[128,2048]{1,0:T(8,128)(2,1)}, bf16[128,2048]{1,0:T(8,128)(2,1)S(1)}, u32[]{:S(2)}) copy-start(bf16[128,2048]{1,0:T(8,128)(2,1)S(1)} %fusion.27) | copy-start | bytes 1572868
  90.1 72.6 %all-gather.3.cloned.1.call-start = ((), (), s32[]{:S(2)}) async-start(), calls=%async_computation.6 | async-start | bytes 2621440 | tf_op jit(solution)/shard_map/all_gather | solution.py:173
  90.8 131.1 %reduce-scatter.8.cloned.1.call-start = ((), (), s32[]{:S(2)}) async-start(), calls=%async_computation.9 | async-start | bytes 7864320 | tf_op jit(solution)/shard_map/reduce_scatter | solution.py:192
  159.4 0.9 copy-start.9
  159.5 1.3 copy-start.13
  159.5 1.4 copy-start.8
  159.5 1.7 copy-start.12
  159.5 108.4 %reduce-scatter.6.cloned.1.call-start = ((), (), s32[]{:S(2)}) async-start(), calls=%async_computation.7 | async-start | bytes 2621440 | tf_op jit(solution)/shard_map/reduce_scatter | solution.py:195
  160.5 2.2 copy-start.7
  162.7 2.5 copy-start.5
  170.1 116.4 %reduce-scatter.4.cloned.1.call-start = ((), (), s32[]{:S(2)}) async-start(), calls=%async_computation.5 | async-start | bytes 1966080 | tf_op jit(solution)/shard_map/reduce_scatter | solution.py:189
  185.9 16.0 %copy-start.6 = (bf16[256,2048]{1,0:T(8,128)(2,1)S(1)}, bf16[256,2048]{1,0:T(8,128)(2,1)}, u32[]{:S(2)}) copy-start(bf16[256,2048]{1,0:T(8,128)(2,1)} %param.23) | copy-start | bytes 3145732
  189.1 3.8 %copy-start.2 = (f32[768,384,4]{1,0,2:T(8,128)S(1)}, f32[768,384,4]{1,0,2:T(8,128)}, u32[]{:S(2)}) copy-start(f32[768,384,4]{1,0,2:T(8,128)} %get-tuple-element.179) | copy-start | bytes 14155780 | tf_op jit(solution)/shard_map/while
  197.1 3.8 %copy-start.2 = (f32[768,384,4]{1,0,2:T(8,128)S(1)}, f32[768,384,4]{1,0,2:T(8,128)}, u32[]{:S(2)}) copy-start(f32[768,384,4]{1,0,2:T(8,128)} %get-tuple-element.179) | copy-start | bytes 14155780 | tf_op jit(solution)/shard_map/while
  203.7 23.0 %copy-start.10 = (s32[128,2]{0,1:T(2,128)S(1)}, s32[128,2]{0,1:T(2,128)}, u32[]{:S(2)}) copy-start(s32[128,2]{0,1:T(2,128)} %param.26) | copy-start | bytes 3076
  203.7 23.1 %copy-start.11 = (f32[128,2]{0,1:T(2,128)S(1)}, f32[128,2]{0,1:T(2,128)}, u32[]{:S(2)}) copy-start(f32[128,2]{0,1:T(2,128)} %param.27) | copy-start | bytes 3076
  221.9 41.4 %all-to-all-start.1 = ((bf16[4,96,2048]{2,1,0:T(8,128)(2,1)}), bf16[4,96,2048]{2,1,0:T(8,128)(2,1)S(1)}, u32[]{:S(2)}, u32[]{:S(2)}) async-start(bf16[4,96,2048]{2,1,0:T(8,128)(2,1)} %bitcast.142), calls=%async_computation.4 | async-start | bytes 3145728 | tf_op jit(solution)/shard_map/all_to_all | solution.py:199
  263.3 1.2 copy-start.4
  264.5 22.0 %copy-start.1 = (bf16[2,256,2048]{2,1,0:T(8,128)(2,1)S(1)}, bf16[2,256,2048]{2,1,0:T(8,128)(2,1)}, u32[]{:S(2)}) copy-start(bf16[2,256,2048]{2,1,0:T(8,128)(2,1)} %param.30) | copy-start | bytes 6291460
Sparse Core Ops, SparseCore 0:
  90.2 45.4 all-gather.4
  137.9 22.5 all-gather.2
  163.0 58.8 reduce-scatter.7
  224.3 31.1 reduce-scatter.5
  258.4 28.0 reduce-scatter.3
where the time goes:
time: 294 us; the launch traced here: 293 us
  waiting for transfers between devices  117 us (40%)
  blocking collectives  58 us (20%)
  local copies, waits for them, and re-layouts  36.6 us (12%)
  matrix products  34.1 us (12%)
  other arithmetic  28.3 us (10%)
  between operations  14.2 us (5%)
  starting transfers between devices  5.02 us (2%)
    all_gather x1, waiting for transfers between devices, body(): lax.all_gather(arrived, 'tp', axis=0, tiled=True)  44.9 us
    all_to_all x1, blocking collectives, body(): lax.all_to_all(outgoing, 'ep', split_axis=1, concat_axis=1, tiled=True)  43.4 us
    all_to_all x1, waiting for transfers between devices, body(): lax.all_to_all(routed_sum.astype(jnp.bfloat16), 'ep', split_axis=0, conca...  36.5 us
    reduce_scatter x1, waiting for transfers between devices, body(): lax.psum_scatter(routed_part.astype(jnp.bfloat16), 'tp', scatter_dimensio...  18.2 us
    reduce_scatter x1, waiting for transfers between devices, body(): lax.psum_scatter(head_partial.astype(jnp.bfloat16), 'tp', scatter_dimensi...  16.3 us
    all_gather x1, blocking collectives, body(): lax.all_gather(keys_and_values, 'ep', axis=0, tiled=True)  14.6 us
    unnamed x34, local copies, waits for them, and re-layouts  14.3 us
    unnamed x4, other arithmetic  12.4 us
  transfers between devices with their start and end apart: 6, of which 4 were waited for; matrix products, arithmetic and copies ran while one was open for 20% of the time, Pallas kernels for 0%

commit v1 on v0

--- a/solution.py
+++ b/solution.py
@@ -175,7 +175,10 @@
     outgoing = jnp.take(
         normed, slot_table(own_slots, slot_count), axis=0, mode="fill", fill_value=0
     )[None]
-    arrived = lax.all_to_all(outgoing, "ep", split_axis=1, concat_axis=1, tiled=True)
+    devices = lax.axis_size("ep")
+    parts = jnp.stack(jnp.split(outgoing, devices, axis=1), axis=0)
+    parts = lax.all_to_all(parts, "ep", split_axis=0, concat_axis=0)
+    arrived = jnp.concatenate(parts, axis=1)
     arrived = arrived.reshape(arrived.shape[0], ep_count, local_experts, capacity, model_width)
     hidden = expert_hidden(
         lax.all_gather(arrived, "tp", axis=0, tiled=True), expert_gate, expert_up

time: 294 us -> 265 us (0.901)
  local copies, waits for them, and re-layouts: 36.6 us -> 23 us
  other arithmetic: 28.3 us -> 16.1 us
  waiting for transfers between devices: 117 us -> 113 us
    unnamed x4 -> x3, other arithmetic: 12.4 us -> 0.01 us
    unnamed x34 -> x24, local copies, waits for them, and re-layouts: 14.3 us -> 2.24 us
    select_n x1 -> x0, local copies, waits for them, and re-layouts: 4.05 us -> none  [body(): jnp.take(normed, slot_table(own_slots, slot_count), axis=0, mode='fill',...]
  transfers between devices with their start and end apart: 6 -> 6, of which waited for: 4 -> 4; matrix products, arithmetic and copies ran while one was open for 20% -> 23% of each run, Pallas kernels for 0% -> 0%
where the time goes in v1:
time: 265 us
  waiting for transfers between devices  113 us (43%)
  blocking collectives  57.7 us (22%)
  matrix products  35.9 us (14%)
  local copies, waits for them, and re-layouts  23 us (9%)
  other arithmetic  16.1 us (6%)
  between operations  14.2 us (5%)
  starting transfers between devices  4.98 us (2%)
    all_gather x1, waiting for transfers between devices, body(): lax.all_gather(arrived, 'tp', axis=0, tiled=True)  44.9 us
    all_to_all x1, blocking collectives, body(): parts = lax.all_to_all(parts, 'ep', split_axis=0, concat_axis=0)  43.1 us
    all_to_all x1, waiting for transfers between devices, body(): lax.all_to_all(routed_sum.astype(jnp.bfloat16), 'ep', split_axis=0, conca...  36.6 us
    reduce_scatter x1, waiting for transfers between devices, body(): lax.psum_scatter(routed_part.astype(jnp.bfloat16), 'tp', scatter_dimensio...  15.9 us
    reduce_scatter x1, waiting for transfers between devices, body(): lax.psum_scatter(head_partial.astype(jnp.bfloat16), 'tp', scatter_dimensi...  14.6 us
    all_gather x1, blocking collectives, body(): lax.all_gather(keys_and_values, 'ep', axis=0, tiled=True)  14.6 us
    dot_general x1, matrix products, body(): jnp.einsum('osjcf,jfd->osjcd', hidden, expert_down, preferred_element_typ...  10.7 us
    convert_element_type x1, local copies, waits for them, and re-layouts, body(): routed_part.astype(jnp.bfloat16)  6.59 us
  transfers between devices with their start and end apart: 6, of which 4 were waited for; matrix products, arithmetic and copies ran while one was open for 23% of the time, Pallas kernels for 0%

profile of v1, /device:TPU:0, one launch (start us, length us, event | category | flops | bytes accessed | tf_op | source)
XLA Modules:
  0.0 264.7 jit_solution(9451065103485733270)
XLA Ops:
  7.2 0.9 copy.70
  8.4 0.6 reduce-window.6
  9.0 0.2 slice_reduce_fusion
  9.4 0.2 fusion.29
  9.7 1.2 fusion.25
  11.0 1.2 fusion.27
  12.2 3.1 %gather_fusion = bf16[384,2048]{1,0:T(8,128)(2,1)} fusion(bf16[128,2048]{1,0:T(8,128)(2,1)S(1)} %fusion.27, s32[1024]{0:T(1024)S(1)} %pad_clamp_fusion.2), kind=kCustom, calls=%fused_computation.2 | custom fusion | bytes 3147264 | tf_op jit(solution)/shard_map/jit(_take)/gather | solution.py:175
  15.4 1.6 bitcast_select_fusion
  17.1 0.2 pad_maximum_fusion
  17.3 43.1 %all_to_all.17 = bf16[4,1,96,2048]{3,2,1,0:T(8,128)(2,1)S(1)} all-to-all(bf16[4,1,96,2048]{3,2,1,0:T(8,128)(2,1)S(1)} %pad_maximum_fusion), channel_id=1, replica_groups=mesh['grp'=2,'ep'=4,'tp'=4] {'ep'}, dimensions={0} | all-to-all | bytes 3145728 | tf_op jit(solution)/shard_map/all_to_all | solution.py:180
  60.4 1.2 copy.73
  61.7 0.7 all-gather.3.cloned.1.call-update
  62.5 44.9 %all-gather.5.cloned.1.call-done = bf16[4,4,2,48,2048]{4,3,1,0,2:T(8,128)(2,1)} async-done(((bf16[1,4,2,48,2048]{4,3,1,0,2:T(8,128)(2,1)}), bf16[4,4,2,48,2048]{4,3,1,0,2:T(8,128)(2,1)}) %all-gather.5.cloned.1.call-update) | async-done | bytes 6291472 | tf_op jit(solution)/shard_map/all_gather | solution.py:184
  107.3 6.4 %fusion.14 = f32[2,4,4,48,256]{4,3,2,1,0:T(8,128)} fusion(bf16[4,4,2,48,2048]{4,3,1,0,2:T(8,128)(2,1)} %all-gather.5.cloned.1.call-done, bf16[2,2048,256]{2,1,0:T(8,128)(2,1)} %param.28), kind=kOutput, calls=%fused_computation.26 | convolution fusion | flops 1610612736 | bytes 9961472 | tf_op jit(solution)/shard_map/osjcd,jdf->osjcf/dot_general | solution.py:100
  113.7 10.7 %convert_bitcast_fusion = bf16[4,4,2,48,2048]{4,3,1,0,2:T(8,128)(2,1)} fusion(bf16[2,256,2048]{2,1,0:T(8,128)(2,1)S(1)} %copy-done, f32[2,4,4,48,256]{4,3,2,1,0:T(8,128)} %fusion.14, bf16[4,4,2,48,2048]{4,3,1,0,2:T(8,128)(2,1)} %all-gather.5.cloned.1.call-done, bf16[2,2048,256]{2,1,0:T(8,128)(2,1)} %param.29), kind=kOutput, calls=%fused_computation.20 | convolution fusion | flops 3226730496 | bytes 18350080 | tf_op jit(solution)/shard_map/osjcf,jfd->osjcd/dot_general | solution.py:186
  124.4 6.6 %copy.74 = bf16[4,4,2,48,2048]{4,3,2,1,0:T(8,128)(2,1)} copy(bf16[4,4,2,48,2048]{4,3,1,0,2:T(8,128)(2,1)} %convert_bitcast_fusion) | data formatting | bytes 12582912 | tf_op jit(solution)/shard_map/convert_element_type | solution.py:196
  131.0 0.2 reduce-scatter.6.cloned.1.call-start
  131.3 0.7 copy-done.6
  131.9 0.2 copy.68
  132.1 0.2 reshape.437
  132.4 0.7 fusion.56
  133.6 0.2 fusion.39
  133.9 0.2 subtract_convert_fusion.1
  134.1 0.2 multiply_multiply_fusion
  134.3 0.5 subtract_convert_fusion
  134.9 2.3 fusion.57
  137.2 5.5 %convolution_convert_fusion = bf16[512,2048]{1,0:T(8,128)(2,1)} fusion(bf16[128,2048]{1,0:T(8,128)(2,1)} %param.33, bf16[512,2048]{1,0:T(8,128)(2,1)} %all-gather.3.cloned.1.call-done, bf16[2048,128]{1,0:T(8,128)(2,1)} %param.32, f32[512,128]{1,0:T(8,128)S(1)} %fusion.57), kind=kOutput, calls=%fused_computation.21 | convolution fusion | flops 538312704 | bytes 5505024 | tf_op jit(solution)/shard_map/dot_general | solution.py:189
  142.7 0.4 pad_maximum_fusion.1
  143.4 0.3 copy-done.5
  143.7 14.6 %all_gather.9 = bf16[1536,128]{0,1:T(8,128)(2,1)S(1)} all-gather(bf16[384,128]{0,1:T(8,128)(2,1)S(1)} %pad_maximum_fusion.2), channel_id=1, replica_groups=mesh['grp'=2,'ep'=4,'tp'=4] {'ep'}, dimensions={0}, use_global_device_ids=true | all-gather | bytes 491520 | tf_op jit(solution)/shard_map/all_gather | solution.py:150
  158.3 0.2 copy.67
  158.5 16.0 %while.15 = (s32[]{:T(128)}, f32[4,384]{1,0:T(4,128)S(1)}, f32[4,384]{1,0:T(4,128)S(1)}, f32[4,384,64]{1,2,0:T(8,128)S(1)}, bf16[2,768,128]{2,1,0:T(8,128)(2,1)S...) while((s32[]{:T(128)}, f32[4,384]{1,0:T(4,128)S(1)}, f32[4,384]{1,0:T(4,128)S(1)}, ...), condition=%wide.region_5.6_spmd.clone, body=%wide.region_2.5_spmd.clone.sunk | while | flops 311729664 | bytes 35094656 | solution.py:89
  158.7 3.0 %bitcast_reduce_fusion.3 = (f32[4,384]{1,0:T(4,128)S(1)}, f32[768,384,4]{1,0,2:T(8,128)}) fusion(bf16[384,4,64]{0,2,1:T(8,128)(2,1)S(1)} %get-tuple-element.201, bf16[768,128]{0,1:T(8,128)(2,1)S(1)} %bitcast.138), kind=kOutput, calls=%fused_computation.4.clone.1 | convolution fusion | flops 153352704 | bytes 5019648 | tf_op jit(solution)/shard_map/while/body/eval_jaxpr/qhd,kd->hqk/dot_general | solution.py:69
  161.8 3.3 %fusion.75 = f32[4,384]{1,0:T(4,128)S(1)} fusion(f32[768,384,4]{1,0,2:T(8,128)} %get-tuple-element.177, f32[4,384]{1,0:T(4,128)S(1)} %select_maximum_fusion.2), kind=kLoop, calls=%fused_computation.7.clone.1 | loop fusion | flops 3537408 | bytes 4730880 | tf_op jit(solution)/shard_map/while/body/eval_jaxpr/reduce_sum | solution.py:80
  165.0 0.5 copy-done.1
  165.5 1.0 fusion.77
  166.7 3.0 %bitcast_reduce_fusion.3 = (f32[4,384]{1,0:T(4,128)S(1)}, f32[768,384,4]{1,0,2:T(8,128)}) fusion(bf16[384,4,64]{0,2,1:T(8,128)(2,1)S(1)} %get-tuple-element.201, bf16[768,128]{0,1:T(8,128)(2,1)S(1)} %bitcast.138), kind=kOutput, calls=%fused_computation.4.clone.1 | convolution fusion | flops 153352704 | bytes 5019648 | tf_op jit(solution)/shard_map/while/body/eval_jaxpr/qhd,kd->hqk/dot_general | solution.py:69
  169.7 3.3 %fusion.75 = f32[4,384]{1,0:T(4,128)S(1)} fusion(f32[768,384,4]{1,0,2:T(8,128)} %get-tuple-element.177, f32[4,384]{1,0:T(4,128)S(1)} %select_maximum_fusion.2), kind=kLoop, calls=%fused_computation.7.clone.1 | loop fusion | flops 3537408 | bytes 4730880 | tf_op jit(solution)/shard_map/while/body/eval_jaxpr/reduce_sum | solution.py:80
  173.0 0.5 copy-done.1
  173.5 1.0 fusion.77
  174.6 3.0 %convolution_convert_fusion.1 = bf16[384,2048]{1,0:T(8,128)(2,1)} fusion(bf16[384,256]{0,1:T(8,128)(2,1)S(1)} %bitcast.143, bf16[256,2048]{1,0:T(8,128)(2,1)} %param.23), kind=kOutput, calls=%fused_computation.22 | convolution fusion | flops 403439616 | bytes 2818048 | tf_op jit(solution)/shard_map/dot_general | solution.py:190
  177.6 15.9 %reduce-scatter.8.cloned.1.call-done = bf16[384,2048]{1,0:T(8,128)(2,1)} async-done(((bf16[1536,2048]{1,0:T(8,128)(2,1)}), bf16[384,2048]{1,0:T(8,128)(2,1)}) %reduce-scatter.8.cloned.1.call-update) | async-done | bytes 1572880 | tf_op jit(solution)/shard_map/reduce_scatter | solution.py:195
  193.5 4.6 %all-to-all-start.1 = ((bf16[4,96,2048]{2,1,0:T(8,128)(2,1)}), bf16[4,96,2048]{2,1,0:T(8,128)(2,1)}, u32[]{:S(2)}, u32[]{:S(2)}) async-start(bf16[4,96,2048]{2,1,0:T(8,128)(2,1)} %bitcast.142), calls=%async_computation.4 | async-start | bytes 3145728 | tf_op jit(solution)/shard_map/all_to_all | solution.py:202
  198.4 36.6 %all-to-all-done.1 = bf16[4,96,2048]{2,1,0:T(8,128)(2,1)} async-done(((bf16[4,96,2048]{2,1,0:T(8,128)(2,1)}), bf16[4,96,2048]{2,1,0:T(8,128)(2,1)}, u32[]{:S(2)}, u32[]{:S(2)}) %all-to-all-start.1) | async-done | bytes 1572896 | tf_op jit(solution)/shard_map/all_to_all | solution.py:202
  235.0 3.1 %gather_fusion.1 = bf16[128,2048]{1,0:T(8,128)(2,1)S(1)} fusion(bf16[384,2048]{1,0:T(8,128)(2,1)} %bitcast.27, s32[1024]{0:T(1024)S(1)} %get-tuple-element.134), kind=kCustom, calls=%fused_computation.clone | custom fusion | bytes 1049088 | tf_op jit(solution)/shard_map/jit(_take)/gather | solution.py:207
  238.1 3.1 %gather_fusion.2 = bf16[128,2048]{1,0:T(8,128)(2,1)S(1)} fusion(bf16[384,2048]{1,0:T(8,128)(2,1)} %bitcast.27, s32[1024]{0:T(1024)S(1)} %get-tuple-element.133), kind=kCustom, calls=%fused_computation.1.clone | custom fusion | bytes 1049088 | tf_op jit(solution)/shard_map/jit(_take)/gather | solution.py:207
  241.2 2.3 add_convert_fusion
  243.5 14.6 %reduce-scatter.4.cloned.1.call-done = bf16[96,2048]{1,0:T(8,128)(2,1)} async-done(((bf16[384,2048]{1,0:T(8,128)(2,1)}), bf16[96,2048]{1,0:T(8,128)(2,1)}) %reduce-scatter.4.cloned.1.call-update) | async-done | bytes 393232 | tf_op jit(solution)/shard_map/reduce_scatter | solution.py:192
  (81 shorter events, 2.6 us)
Async XLA Ops:
  7.2 106.5 %copy-start = (bf16[2,256,2048]{2,1,0:T(8,128)(2,1)S(1)}, bf16[2,256,2048]{2,1,0:T(8,128)(2,1)}, u32[]{:S(2)}) copy-start(bf16[2,256,2048]{2,1,0:T(8,128)(2,1)} %param.30) | copy-start | bytes 6291460
  7.2 100.1 %all-gather.5.cloned.1.call-start = ((), (), s32[]{:S(2)}) async-start(), calls=%async_computation.8 | async-start | bytes 7864320 | tf_op jit(solution)/shard_map/all_gather | solution.py:184
  12.2 3.1 %copy-start.2 = (bf16[128,2048]{1,0:T(8,128)(2,1)}, bf16[128,2048]{1,0:T(8,128)(2,1)S(1)}, u32[]{:S(2)}) copy-start(bf16[128,2048]{1,0:T(8,128)(2,1)S(1)} %fusion.27) | copy-start | bytes 1572868
  61.7 73.2 %all-gather.3.cloned.1.call-start = ((), (), s32[]{:S(2)}) async-start(), calls=%async_computation.6 | async-start | bytes 2621440 | tf_op jit(solution)/shard_map/all_gather | solution.py:173
  62.4 131.1 %reduce-scatter.8.cloned.1.call-start = ((), (), s32[]{:S(2)}) async-start(), calls=%async_computation.9 | async-start | bytes 7864320 | tf_op jit(solution)/shard_map/reduce_scatter | solution.py:195
  131.0 0.9 copy-start.6
  131.0 1.3 copy-start.10
  131.0 1.4 copy-start.4
  131.0 2.3 copy-start.9
  131.0 110.2 %reduce-scatter.6.cloned.1.call-start = ((), (), s32[]{:S(2)}) async-start(), calls=%async_computation.7 | async-start | bytes 2621440 | tf_op jit(solution)/shard_map/reduce_scatter | solution.py:198
  132.1 2.8 %copy-start.3 = (bf16[2048,128]{1,0:T(8,128)(2,1)S(1)}, bf16[2048,128]{1,0:T(8,128)(2,1)}, u32[]{:S(2)}) copy-start(bf16[2048,128]{1,0:T(8,128)(2,1)} %param.31) | copy-start | bytes 1572868
  142.7 1.0 copy-start.5
  142.7 115.4 %reduce-scatter.4.cloned.1.call-start = ((), (), s32[]{:S(2)}) async-start(), calls=%async_computation.5 | async-start | bytes 1966080 | tf_op jit(solution)/shard_map/reduce_scatter | solution.py:192
  161.8 3.8 %copy-start.1 = (f32[768,384,4]{1,0,2:T(8,128)S(1)}, f32[768,384,4]{1,0,2:T(8,128)}, u32[]{:S(2)}) copy-start(f32[768,384,4]{1,0,2:T(8,128)} %get-tuple-element.177) | copy-start | bytes 14155780 | tf_op jit(solution)/shard_map/while
  169.7 3.8 %copy-start.1 = (f32[768,384,4]{1,0,2:T(8,128)S(1)}, f32[768,384,4]{1,0,2:T(8,128)}, u32[]{:S(2)}) copy-start(f32[768,384,4]{1,0,2:T(8,128)} %get-tuple-element.177) | copy-start | bytes 14155780 | tf_op jit(solution)/shard_map/while
  177.6 20.7 %copy-start.7 = (s32[128,2]{0,1:T(2,128)S(1)}, s32[128,2]{0,1:T(2,128)}, u32[]{:S(2)}) copy-start(s32[128,2]{0,1:T(2,128)} %param.26) | copy-start | bytes 3076
  177.6 20.8 %copy-start.8 = (f32[128,2]{0,1:T(2,128)S(1)}, f32[128,2]{0,1:T(2,128)}, u32[]{:S(2)}) copy-start(f32[128,2]{0,1:T(2,128)} %param.27) | copy-start | bytes 3076
  193.5 41.5 %all-to-all-start.1 = ((bf16[4,96,2048]{2,1,0:T(8,128)(2,1)}), bf16[4,96,2048]{2,1,0:T(8,128)(2,1)}, u32[]{:S(2)}, u32[]{:S(2)}) async-start(bf16[4,96,2048]{2,1,0:T(8,128)(2,1)} %bitcast.142), calls=%async_computation.4 | async-start | bytes 3145728 | tf_op jit(solution)/shard_map/all_to_all | solution.py:202
Sparse Core Ops, SparseCore 0:
  61.8 45.4 all-gather.4
  109.5 22.5 all-gather.2
  134.6 58.8 reduce-scatter.7
  195.9 31.1 reduce-scatter.5
  230.0 28.0 reduce-scatter.3
